TPU v7x, 32 devices: a whole 2x2x4 slice. The times are simulated.
32 devices in a mesh: sp: 8 (over z, y), tp: 4 (over x, core).
Axes of the slice: x: 2, y: 2, z: 4, core: 2. Of those that a mesh axis runs over, the one named last changes fastest.
Arguments:
- tokens: bfloat16 [4, 4096, 2048], P(None, ('sp', 'tp')), may hold values from -6 to 6
- in_gain: float32 [2048], replicated, may hold values from 0.1 to 1.9
- query_weight: bfloat16 [2048, 1024], P(None, 'tp'), may hold values from -0.125 to 0.125
- key_weight: bfloat16 [2048, 1024], P(None, 'tp'), may hold values from -0.125 to 0.125
- value_weight: bfloat16 [2048, 1024], P(None, 'tp'), may hold values from -0.125 to 0.125
- gate_weight: bfloat16 [2048, 1024], P(None, 'tp'), may hold values from -0.125 to 0.125
- log_decay: float32 [8], P('tp'), may hold values from -0.034 to 0, as said below
- norm_gain: float32 [1024], P('tp'), may hold values from 0.1 to 1.9
- out_weight: bfloat16 [1024, 2048], replicated, may hold values from -0.1875 to 0.1875
- post_gain: float32 [2048], replicated, may hold values from 0.1 to 1.9
Outputs:
- mixed: bfloat16 [4, 4096, 2048], P(None, ('sp', 'tp'))
Inputs may be any that keep to these rules, and one draw needn't show every extreme that they name: `log_decay`: every entry is negative; some heads keep a tenth or more of their memory over 4096 positions, others lose most of it within 30 to 100 positions.
All inputs are finite; a program needn't handle non-finite values.
Results may differ from a plain program's by a relative error of at most 0.015.
Values may be sent and summed in bfloat16 or wider, within the bound.
A program may use at most 64 MiB of HBM per device.

v0:
```python
import jax
import jax.numpy as jnp
from jax import lax
from jax.sharding import PartitionSpec as P

HEAD_DIM = 128
BLOCK = 128


rms_eps = 1e-06
group_eps = 1e-05
rope_base = 10000.0


def carried_in(value, axis, join, neutral):
    count, mine = (lax.axis_size(axis), lax.axis_index(axis))
    pieces = jax.tree.map(lambda part: lax.all_gather(part, axis), value)
    running = jax.tree.map(
        lambda part, zero: jnp.full_like(part, 0) + jnp.asarray(zero, part.dtype), value, neutral
    )

    def lap(position, running):
        longer = join(running, jax.tree.map(lambda part: part[position], pieces))
        return jax.tree.map(lambda new, old: jnp.where(position < mine, new, old), longer, running)

    return lax.fori_loop(0, count - 1, lap, running)


def rotate(values, positions):
    half_dim = values.shape[-1] // 2
    inverse = rope_base ** (-jnp.arange(half_dim, dtype=jnp.float32) / half_dim)
    angles = positions.astype(jnp.float32)[:, None] * inverse[None, :]
    cosine = jnp.cos(angles)
    sine_part = jnp.sin(angles)
    first_half = values[..., :half_dim].astype(jnp.float32)
    second = values[..., half_dim:].astype(jnp.float32)
    return jnp.concatenate(
        [first_half * cosine - second * sine_part, first_half * sine_part + second * cosine],
        axis=-1,
    )


def local_pass(queries, key_rows, values, log_decay):
    seq_count, head_count, length, head_width = queries.shape
    block_count = length // BLOCK
    offsets = jnp.arange(BLOCK, dtype=jnp.float32)
    distance = offsets[:, None] - offsets[None, :]
    rate_col = log_decay[:, None, None]
    inside = jnp.where(distance >= 0, jnp.exp(rate_col * jnp.maximum(distance, 0.0)), 0.0)
    query_scale = jnp.exp(log_decay[:, None] * (offsets + 1.0))[..., None]
    key_scale = jnp.exp(log_decay[:, None] * (BLOCK - 1.0 - offsets))[..., None]
    block_decay = jnp.exp(log_decay * BLOCK)[:, None, None]

    def to_blocks(arr):
        return arr.reshape(seq_count, head_count, block_count, BLOCK, arr.shape[-1]).transpose(
            2, 0, 1, 3, 4
        )

    def advance(memory, inputs):
        q_block, k_block, v_block = inputs
        scores = jnp.einsum("shqd,shkd->shqk", q_block, k_block, preferred_element_type=jnp.float32)
        weights = (scores * inside).astype(jnp.bfloat16)
        within = jnp.einsum("shqk,shkv->shqv", weights, v_block, preferred_element_type=jnp.float32)
        carried = jnp.einsum(
            "shqd,shdv->shqv",
            q_block.astype(jnp.float32) * query_scale,
            memory,
            precision=lax.Precision.HIGHEST,
        )
        k_scaled = (k_block.astype(jnp.float32) * key_scale).astype(jnp.bfloat16)
        memory = memory * block_decay + jnp.einsum(
            "shkd,shkv->shdv", k_scaled, v_block, preferred_element_type=jnp.float32
        )
        return (memory, within + carried)

    start_memory = jnp.zeros((seq_count, head_count, head_width, values.shape[-1]), jnp.float32)
    end_state, outputs = lax.scan(
        advance, start_memory, (to_blocks(queries), to_blocks(key_rows), to_blocks(values))
    )
    outputs = outputs.transpose(1, 2, 0, 3, 4).reshape(
        seq_count, head_count, length, values.shape[-1]
    )
    return (outputs, end_state)


def combine(earlier, later_part):
    return (
        earlier[0] * later_part[0],
        earlier[1] * later_part[0][None, :, None, None] + later_part[1],
    )


def read_out(carried, queries, partial_out, log_decay):
    length = queries.shape[2]
    read_scale = jnp.exp(log_decay[:, None] * (jnp.arange(length, dtype=jnp.float32) + 1.0))[
        ..., None
    ]
    return partial_out + jnp.einsum(
        "shld,shdv->shlv",
        queries.astype(jnp.float32) * read_scale,
        carried,
        precision=lax.Precision.HIGHEST,
    )


def body(
    tokens,
    in_gain,
    query_weight,
    key_weight,
    value_weight,
    gate_weight,
    log_decay,
    norm_gain,
    out_weight,
    post_gain,
):
    seq_count, rows_dev, model_width = tokens.shape
    tp_size = lax.axis_size("tp")
    local_width = query_weight.shape[1]
    head_count = local_width // HEAD_DIM
    stretch = rows_dev * tp_size
    tok_f32 = tokens.astype(jnp.float32)
    normed = (
        tok_f32 * lax.rsqrt(jnp.mean(tok_f32 * tok_f32, axis=-1, keepdims=True) + rms_eps) * in_gain
    ).astype(jnp.bfloat16)
    joined = jnp.concatenate([query_weight, key_weight, value_weight, gate_weight], axis=1)
    projected = jnp.einsum(
        "kux,xt->kut",
        lax.all_gather(normed, "tp", axis=1, tiled=True),
        joined,
        preferred_element_type=jnp.float32,
    ).astype(jnp.bfloat16)

    def heads_of(columns):
        return columns.reshape(seq_count, stretch, head_count, HEAD_DIM).transpose(0, 2, 1, 3)

    positions = lax.axis_index("sp") * stretch + jnp.arange(stretch, dtype=jnp.int32)
    queries = rotate(heads_of(projected[..., :local_width]), positions).astype(jnp.bfloat16)
    key_rows = (
        rotate(heads_of(projected[..., local_width : 2 * local_width]), positions)
        * HEAD_DIM ** (-0.5)
    ).astype(jnp.bfloat16)
    values = heads_of(projected[..., 2 * local_width : 3 * local_width])
    gating = projected[..., 3 * local_width :]
    partial_out, end_state = local_pass(queries, key_rows, values, log_decay)
    span_decay = jnp.exp(log_decay * stretch)
    carried = carried_in(
        (span_decay, end_state),
        "sp",
        combine,
        (jnp.ones_like(span_decay), jnp.zeros_like(end_state)),
    )[1]
    retained = read_out(carried, queries, partial_out, log_decay)
    center = jnp.mean(retained, axis=-1, keepdims=True)
    spread = jnp.mean(jnp.square(retained - center), axis=-1, keepdims=True)
    normal = (
        ((retained - center) * lax.rsqrt(spread + group_eps))
        .transpose(0, 2, 1, 3)
        .reshape(seq_count, stretch, local_width)
    )
    gated = (normal * norm_gain * jax.nn.silu(gating.astype(jnp.float32))).astype(jnp.bfloat16)
    premix = jnp.einsum(
        "hor,rn->hon",
        lax.all_to_all(gated, "tp", split_axis=1, concat_axis=2, tiled=True),
        out_weight,
        preferred_element_type=jnp.float32,
    )
    mixed = (
        premix * lax.rsqrt(jnp.mean(premix * premix, axis=-1, keepdims=True) + rms_eps) * post_gain
    )
    return mixed.astype(jnp.bfloat16)


def solution(mesh):
    placed = (
        P(None, ("sp", "tp"), None),
        P(),
        P(None, "tp"),
        P(None, "tp"),
        P(None, "tp"),
        P(None, "tp"),
        P("tp"),
        P("tp"),
        P(),
        P(),
    )
    return jax.shard_map(
        body, mesh=mesh, in_specs=placed, out_specs=P(None, ("sp", "tp"), None), check_vma=False
    )
```

profile of v0, /device:TPU:25, one launch (start us, length us, event | category | flops | bytes accessed | tf_op | source)
XLA Modules:
  0.0 246.2 jit_solution(14427455842791182812)
XLA Ops:
  6.5 2.2 fusion.40
  8.8 2.6 %fusion.42 = bf16[4,128,2048]{2,1,0:T(8,128)(2,1)} fusion(bf16[4,128,2048]{2,1,0:T(8,128)(2,1)S(1)} %copy-done.1, f32[2048]{0:T(1024)} %param.15, f32[4,128]{1,0:T(4,128)S(1)} %add_rsqrt_fusion.2), kind=kLoop, calls=%fused_computation.45 | loop fusion | flops 4194304 | bytes 4204544 | tf_op jit(solution)/shard_map/convert_element_type | solution.py:126
  14.2 57.0 %all-gather.5.cloned.1.call-done = bf16[4,512,2048]{2,1,0:T(8,128)(2,1)} async-done(((bf16[4,128,2048]{2,1,0:T(8,128)(2,1)}), bf16[4,512,2048]{2,1,0:T(8,128)(2,1)}) %all-gather.5.cloned.1.call-update) | async-done | bytes 8388624 | tf_op jit(solution)/shard_map/all_gather | solution.py:130
  71.2 11.8 %fusion.52 = bf16[4,512,1024]{2,1,0:T(8,128)(2,1)S(1)} fusion(bf16[4,512,2048]{2,1,0:T(8,128)(2,1)} %all-gather.5.cloned.1.call-done, bf16[2048,256]{1,0:T(8,128)(2,1)S(1)} %copy-done.9, bf16[2048,256]{1,0:T(8,128)(2,1)S(1)} %copy-done.10, bf16[2048,256]{1,0:T(8,128)(2,1)} %param.17, bf16[2048,256]{1,0:T(8,128)(2,1)} %param.16), kind=kOutput, calls=%fused_computation.58 | convolution fusion | flops 8608808960 | bytes 16777216 | tf_op jit(solution)/shard_map/kux,xt->kut/dot_general | solution.py:128
  83.1 2.0 fusion.80
  88.6 3.2 %fusion.68 = (bf16[4,2,512,64]{2,3,1,0:T(8,128)(2,1)S(1)}, bf16[4,2,512,64]{2,3,1,0:T(8,128)(2,1)S(1)}, f32[4,2,512,64]{2,3,1,0:T(8,128)}, f32[4,2,512,64]{2,3,1,0:T(8,128)}) fusion(f32[512,64]{0,1:T(8,128)S(1)} %get-tuple-element.360, f32[512,64]{0,1:T(8,128)S(1)} %get-tuple-element.359, bf16[4,2,512,128]{2,3,1,0:T(8,128)(2,1)} %bitcast.117, ...), kind=kLoop, calls=%fused_computation.85 | loop fusion | flops 4718592 | bytes 5505024 | tf_op jit(solution)/shard_map/convert.5
  92.9 1.7 maximum_bitcast_fusion.4
  97.0 2.6 %concatenate.25 = f32[4,2,4,128,64]{3,2,4,1,0:T(4,128)} reshape(f32[4,2,512,64]{2,3,1,0:T(8,128)} %get-tuple-element.357) | data formatting | bytes 2097152 | tf_op jit(solution)/shard_map/concatenate | solution.py:37
  99.6 2.9 %fusion.71 = bf16[4,4,2,128,128]{3,0,4,2,1:T(4,128)(2,1)} fusion(f32[4,2,4,128,64]{3,2,4,1,0:T(4,128)} %concatenate.25, f32[4,2,4,128,64]{3,2,4,1,0:T(4,128)S(1)} %concatenate.24), kind=kLoop, calls=%fused_computation.88 | loop fusion | flops 1572864 | bytes 3145728 | tf_op jit(solution)/shard_map/transpose | solution.py:55
  102.5 1.7 copy.32
  104.2 2.4 copy.51
  106.6 17.7 %while.30 = (s32[]{:T(128)}, f32[4,2,128,128]{3,2,1,0:T(8,128)S(1)}, f32[4,4,2,128,128]{4,3,2,1,0:T(8,128)}, f32[2]{0:T(128)S(1)}, bf16[4,4,2,128,128]{4,3,2,1,0...) while((s32[]{:T(128)}, ...), condition=%wide.region_2.3_spmd.clone.clone.clone, body=%wide.region_1.2_spmd.clone.clone.clone.sunk | while | flops 303628800 | bytes 5072032 | solution.py:77
  125.2 14.4 %all-reduce = f32[16]{0:T(128)S(1)} all-reduce(f32[16]{0:T(128)S(1)} %get-tuple-element.361), channel_id=2, replica_groups=mesh['sp'=8,'tp'=4] {'sp'}, use_global_device_ids=true, to_apply=%add | all-reduce | flops 16 | bytes 128
  139.8 2.9 %copy.35 = f32[4,2,4,128,128]{3,2,4,1,0:T(4,128)} copy(f32[4,2,4,128,128]{4,3,1,0,2:T(8,128)} %bitcast.118) | data formatting | bytes 4194304 | tf_op jit(solution)/shard_map/transpose | solution.py:80
  142.7 2.1 reshape.188
  144.8 51.5 %all-gather.7.cloned.1.call-done = f32[32,2,128,128]{3,2,1,0:T(8,128)} async-done(((f32[4,2,128,128]{3,2,1,0:T(8,128)}), f32[32,2,128,128]{3,2,1,0:T(8,128)}) %all-gather.7.cloned.1.call-update) | async-done | bytes 4194320 | tf_op jit(solution)/shard_map/all_gather | solution.py:17
  196.3 8.5 %while.29 = (s32[]{:T(128)}, f32[4,2,128,128]{3,2,1,0:T(8,128)S(1)}, s32[]{:T(128)}, f32[8,2]{1,0:T(8,128)S(1)}, f32[8,4,2,128,128]{4,3,2,1,0:T(8,128)}, /*index=5*/s32[]{:T(128)}, s32[]{:T(128)}) while((s32[]{:T(128)}, f32[4,2,128,128]{3,2,1,0:T(8,128)S(1)}, s32[]{:T(128)}, f32[8,2]{1,0:T(8,128)S(1)}, ...), condition=%wide.region_4.5_spmd.clone, body=%wide.region_3.4_spmd.clone.sunk | while | flops 524292 | bytes 1572993 | solution.py:26
  204.9 3.3 %fusion.81 = (f32[4,2,512]{2,1,0:T(2,128)S(1)}, f32[4,2,512,128]{2,3,1,0:T(8,128)S(1)}) fusion(f32[4,2,512,128]{2,3,1,0:T(8,128)S(1)} %reshape.188, f32[4,2,128,128]{3,2,1,0:T(8,128)S(1)} %get-tuple-element.154, bf16[4,2,512,64]{2,3,1,0:T(8,128)(2,1)} %copy-done.4, bf16[4,2,512,64]{2,3,1,0:T(8,128)(2,1)S(1)} %copy-done.3, ...), kind=kOutput, calls=%fused_computation.117 | convolution fusion | flops 808972288 | bytes 5787648 | tf_op jit(solution)/shard_map/shld,shdv->shlv/dot_general | solution.py:98
  208.5 1.6 subtract_multiply_fusion
  210.1 1.9 copy.46
  212.0 1.9 fusion.61
  214.7 16.7 %all_to_all.18 = bf16[4,512,256]{2,0,1:T(4,128)(2,1)S(1)} all-to-all(bf16[4,512,256]{2,0,1:T(4,128)(2,1)S(1)} %copy.39), channel_id=1, replica_groups=mesh['sp'=8,'tp'=4] {'tp'}, dimensions={1} | all-to-all | bytes 2097152 | tf_op jit(solution)/shard_map/all_to_all | solution.py:165
  233.0 4.6 %multiply_reduce_fusion = (f32[4,128]{1,0:T(4,128)S(1)}, f32[4,128,2048]{2,1,0:T(8,128)S(1)}) fusion(bf16[4,128,1024]{2,1,0:T(8,128)(2,1)S(1)} %all_to_all.16, bf16[1024,2048]{1,0:T(8,128)(2,1)} %param.22), kind=kOutput, calls=%fused_computation.57 | convolution fusion | flops 2149580288 | bytes 9439232 | tf_op jit(solution)/shard_map/hor,rn->hon/dot_general | solution.py:163
  237.6 1.7 multiply_convert_fusion.2
  (91 shorter events, 38.6 us)
Async XLA Ops:
  6.5 2.2 copy-start.1
  6.5 64.7 %all-gather.5.cloned.1.call-start = ((), (), s32[]{:S(2)}) async-start(), calls=%async_computation.1 | async-start | bytes 10485760 | tf_op jit(solution)/shard_map/all_gather | solution.py:130
  11.4 0.7 copy-start.11
  11.4 2.1 copy-start.6
  11.4 59.8 %copy-start.9 = (bf16[2048,256]{1,0:T(8,128)(2,1)S(1)}, bf16[2048,256]{1,0:T(8,128)(2,1)}, u32[]{:S(2)}) copy-start(bf16[2048,256]{1,0:T(8,128)(2,1)} %param.19) | copy-start | bytes 3145732
  11.4 59.8 %copy-start.10 = (bf16[2048,256]{1,0:T(8,128)(2,1)S(1)}, bf16[2048,256]{1,0:T(8,128)(2,1)}, u32[]{:S(2)}) copy-start(bf16[2048,256]{1,0:T(8,128)(2,1)} %param.18) | copy-start | bytes 3145732
  11.4 184.9 %all-gather.7.cloned.1.call-start = ((), (), s32[]{:S(2)}) async-start(), calls=%async_computation.2 | async-start | bytes 4718592 | tf_op jit(solution)/shard_map/all_gather | solution.py:17
  83.1 2.6 %copy-start.5 = (bf16[4,512,1024]{2,1,0:T(8,128)(2,1)}, bf16[4,512,1024]{2,1,0:T(8,128)(2,1)S(1)}, u32[]{:S(2)}) copy-start(bf16[4,512,1024]{2,1,0:T(8,128)(2,1)S(1)} %fusion.52) | copy-start | bytes 12582916
  91.8 1.1 copy-start.2
  91.8 1.1 copy-start.4
  124.4 0.8 copy-start
  196.3 8.6 %copy-start.3 = (bf16[4,2,512,64]{2,3,1,0:T(8,128)(2,1)S(1)}, bf16[4,2,512,64]{2,3,1,0:T(8,128)(2,1)}, u32[]{:S(2)}) copy-start(bf16[4,2,512,64]{2,3,1,0:T(8,128)(2,1)} %copy-done.2) | copy-start | bytes 1572868
  210.1 1.9 copy-start.8
  233.0 4.6 %copy-start.7 = (f32[2048]{0:T(1024)S(1)}, f32[2048]{0:T(1024)}, u32[]{:S(2)}) copy-start(f32[2048]{0:T(1024)} %param.23) | copy-start | bytes 24580
Sparse Core Ops, SparseCore 0:
  11.5 59.6 all-gather.4
  125.3 70.9 all-gather.6
where the time goes:
time: 251 us; the launch traced here: 246 us
  waiting for transfers between devices  109 us (43%)
  matrix products  36.7 us (15%)
  blocking collectives  31.1 us (12%)
  other arithmetic  27.9 us (11%)
  local copies, waits for them, and re-layouts  27.2 us (11%)
  between operations  14.4 us (6%)
    all_gather x1, waiting for transfers between devices, body(): lax.all_gather(normed, 'tp', axis=1, tiled=True)  57 us
    all_gather x1, waiting for transfers between devices, carried_in(): pieces = jax.tree.map(lambda part: lax.all_gather(part, axis), value)  51.5 us
    all_to_all x1, blocking collectives, body(): lax.all_to_all(gated, 'tp', split_axis=1, concat_axis=2, tiled=True)  16.7 us
    unnamed x1, blocking collectives  14.4 us
    dot_general x1, matrix products, body(): jnp.einsum('kux,xt->kut', lax.all_gather(normed, 'tp', axis=1, tiled=True...  11.8 us
    select_n x7, other arithmetic, lap(): jnp.where(position < mine, new, old)  8.26 us
    dot_general x4, matrix products, advance(): jnp.einsum('shqd,shdv->shqv', q_block.astype(jnp.float32) * query_scale,...  6.11 us
    dot_general x4, matrix products, advance(): jnp.einsum('shqk,shkv->shqv', weights, v_block, preferred_element_type=jn...  5.53 us
  transfers between devices with their start and end apart: 2, of which 2 were waited for; matrix products, arithmetic and copies ran while one was open for 3% of the time, Pallas kernels for 0%

commit v1 on v0

v1 whole, which is shorter than its diff:
```python
import functools
import math

import jax
import jax.numpy as jnp
import numpy as np
from jax import lax
from jax.experimental import pallas as pl
from jax.experimental.pallas import tpu as pltpu
from jax.sharding import PartitionSpec as P

HEAD_DIM = 128
SUB = 128
rms_eps = 1e-06
group_eps = 1e-05
rope_base = 10000.0
MESH = pl.DeviceIdType.MESH
F32 = jnp.float32
BF16 = jnp.bfloat16


def kernel(
    tp, sp,
    tok, gain, wq_h, wk_h, wv_h, wg_h, decay, ngain, wo_h, pgain, inv,
    out,
    gath, wq, wk, wv, wg, wo, nb, cosv, sinv, mask, qs, ks, vs, gs,
    within, state, excl, st_out, st_in, g_out, g_in, premix,
    x_send, p_send, t_recv, s_send, s_recv, g_send, g_recv, w_sem, own_sem,
):
    seqs, rows, width = tok.shape
    length = rows * tp
    cols = wq.shape[1]
    heads = cols // HEAD_DIM
    chips = tp // 2
    pair = 2 * rows
    rounds = [1 << k for k in range(max(1, (sp - 1).bit_length()))] if sp > 1 else []
    last = len(rounds) - 1
    s, t = lax.axis_index("sp"), lax.axis_index("tp")
    chip, core = lax.div(t, 2), lax.rem(t, 2)
    other = chip * 2 + 1 - core

    barrier = pltpu.get_barrier_semaphore()
    for j in range(1, tp):
        pl.semaphore_signal(
            barrier, inc=1, device_id={"tp": lax.rem(t + j, tp)}, device_id_type=MESH
        )
    for d in rounds:
        @pl.when(s + d < sp)
        def _():
            pl.semaphore_signal(barrier, inc=1, device_id={"sp": s + d}, device_id_type=MESH)

        @pl.when(s >= d)
        def _():
            pl.semaphore_signal(barrier, inc=1, device_id={"sp": s - d}, device_id_type=MESH)

    peers = jnp.int32(tp - 1)
    for d in rounds:
        peers = peers + jnp.where(s + d < sp, 1, 0) + jnp.where(s >= d, 1, 0)
    pl.semaphore_wait(barrier, peers)

    def block(q, who):
        return gath.at[q, pl.ds(pl.multiple_of(who * rows, rows), rows), :]

    def to_chip(q, j):
        peer = lax.rem(chip + j, chips) * 2 + core
        return pltpu.make_async_remote_copy(
            tok.at[q], block(q, t), x_send.at[q, j], t_recv.at[q, t],
            device_id={"tp": peer}, device_id_type=MESH,
        )

    def to_core(q, who, mine):
        return pltpu.make_async_remote_copy(
            tok.at[q] if mine else block(q, who), block(q, who),
            p_send.at[q, who], t_recv.at[q, who],
            device_id={"tp": other}, device_id_type=MESH,
        )

    def arrived(q, who):
        pltpu.make_async_remote_copy(
            tok.at[q], block(q, who), p_send.at[q, who], t_recv.at[q, who],
            device_id={"tp": other}, device_id_type=MESH,
        ).wait_recv()

    for q in range(seqs):
        for j in range(1, chips):
            to_chip(q, j).start()
    own = [pltpu.make_async_copy(tok.at[q], block(q, t), own_sem.at[q]) for q in range(seqs)]
    for q in range(seqs):
        own[q].start()
        to_core(q, t, True).start()
    loads = [
        pltpu.make_async_copy(a, b, w_sem.at[i])
        for i, (a, b) in enumerate(
            ((wq_h, wq), (wk_h, wk), (wv_h, wv), (wg_h, wg), (wo_h, wo))
        )
    ]
    for load in loads:
        load.start()

    place = (s * length + lax.broadcasted_iota(jnp.int32, (length, HEAD_DIM), 0)).astype(F32)
    angle = place * inv[...]
    cosv[...] = jnp.cos(angle)
    lane = lax.broadcasted_iota(jnp.int32, (length, HEAD_DIM), 1)
    sine = jnp.sin(angle)
    sinv[...] = jnp.where(lane < HEAD_DIM // 2, -sine, sine)
    for h in range(heads):
        def fill(i, _):
            at = pl.multiple_of(i * 32, 32)
            gap = (
                at + lax.broadcasted_iota(jnp.int32, (32, length), 0)
                - lax.broadcasted_iota(jnp.int32, (32, length), 1)
            )
            weight = jnp.exp(decay[h] * jnp.maximum(gap, 0).astype(F32))
            mask[h, pl.ds(at, 32), :] = jnp.where(gap >= 0, weight, 0.0)
            return 0

        lax.fori_loop(0, length // 32, fill, 0)
    excl[...] = jnp.zeros_like(excl)

    def head(h):
        return slice(h * HEAD_DIM, (h + 1) * HEAD_DIM)

    def project(q, which):
        base = pl.multiple_of(which * pair, pair)

        def norm(i, _):
            at = pl.multiple_of(i * 16, 16)
            x = gath[q, pl.ds(pl.multiple_of(base + at, 16), 16), :].astype(F32)
            scale = lax.rsqrt(jnp.mean(x * x, axis=-1, keepdims=True) + rms_eps)
            nb[pl.ds(at, 16), :] = (x * scale * gain[...]).astype(BF16)
            return 0

        lax.fori_loop(0, pair // 16, norm, 0)
        span = pl.ds(base, pair)
        for w, dest, kind in ((wk, ks, 2), (wv, vs, 0), (wq, qs, 1), (wg, gs, 0)):
            r = jnp.dot(nb[...], w[...], preferred_element_type=F32).astype(BF16)
            if kind == 0:
                dest[q, span, :] = r
            else:
                for h in range(heads):
                    x = r[:, head(h)].astype(F32)
                    x = x * cosv[span, :] + pltpu.roll(x, HEAD_DIM // 2, 1) * sinv[span, :]
                    if kind == 2:
                        x = x * HEAD_DIM ** (-0.5)
                    dest[q, span, head(h)] = x.astype(BF16)

    def send_state(q, k):
        for h in range(heads):
            total = state[q, h] + jnp.exp(jnp.full((1, 1), decay[h] * length, F32)) * excl[q, h]
            st_out[q, k, h] = total.astype(BF16)

        @pl.when(s + rounds[k] < sp)
        def _():
            state_copy(q, k).start()

    def state_copy(q, k):
        return pltpu.make_async_remote_copy(
            st_out.at[q, k], st_in.at[q, k], s_send.at[q, k], s_recv.at[q, k],
            device_id={"sp": lax.rem(s + rounds[k], sp)}, device_id_type=MESH,
        )

    def take_state(q, k):
        @pl.when(s >= rounds[k])
        def _():
            state_copy(q, k).wait_recv()
            for h in range(heads):
                rate = jnp.exp(jnp.full((1, 1), decay[h] * (length * (rounds[k] - 1)), F32))
                excl[q, h] += rate * st_in[q, k, h].astype(F32)

    def make_state(q):
        spot = lax.broadcasted_iota(jnp.int32, (length, HEAD_DIM), 0)
        for h in range(heads):
            fade = jnp.exp(decay[h] * (length - 1 - spot).astype(F32))
            scaled = (ks[q, :, head(h)].astype(F32) * fade).astype(BF16)
            state[q, h] = lax.dot_general(
                scaled, vs[q, :, head(h)], (((0,), (0,)), ((), ())), preferred_element_type=F32
            )

    def inside(q):
        for h in range(heads):
            for i in range(length // SUB):
                here, upto = slice(i * SUB, (i + 1) * SUB), slice(0, (i + 1) * SUB)
                score = lax.dot_general(
                    qs[q, here, head(h)], ks[q, upto, head(h)],
                    (((1,), (1,)), ((), ())), preferred_element_type=F32,
                )
                weight = (score * mask[h, here, upto]).astype(BF16)
                within[q, here, head(h)] = jnp.dot(
                    weight, vs[q, upto, head(h)], preferred_element_type=F32
                )

    def gated_copy(q, j):
        dest = lax.rem(t + j, tp)
        return pltpu.make_async_remote_copy(
            g_out.at[q, pl.ds(pl.multiple_of(dest * rows, rows), rows), :],
            g_in.at[q, :, pl.ds(pl.multiple_of(t * cols, cols), cols)],
            g_send.at[q, j], g_recv.at[q, j],
            device_id={"tp": dest}, device_id_type=MESH,
        )

    def gated_own(q):
        return pltpu.make_async_copy(
            g_out.at[q, pl.ds(pl.multiple_of(t * rows, rows), rows), :],
            g_in.at[q, :, pl.ds(pl.multiple_of(t * cols, cols), cols)],
            g_recv.at[q, 0],
        )

    def finish(q):
        for h in range(heads):
            memory = excl[q, h].astype(BF16)
            for i in range(length // SUB):
                here = slice(i * SUB, (i + 1) * SUB)
                spot = i * SUB + 1 + lax.broadcasted_iota(jnp.int32, (SUB, HEAD_DIM), 0)
                reach = jnp.exp(decay[h] * spot.astype(F32))
                query = (qs[q, here, head(h)].astype(F32) * reach).astype(BF16)
                kept = within[q, here, head(h)] + jnp.dot(
                    query, memory, preferred_element_type=F32
                )
                kept = kept - jnp.mean(kept, axis=-1, keepdims=True)
                spread = jnp.mean(kept * kept, axis=-1, keepdims=True)
                normal = kept * lax.rsqrt(spread + group_eps) * ngain[:, head(h)]
                gate = gs[q, here, head(h)].astype(F32)
                g_out[q, here, head(h)] = (normal * (gate * jax.nn.sigmoid(gate))).astype(BF16)
        for j in range(1, tp):
            gated_copy(q, j).start()
        gated_own(q).start()

    def emit(q):
        for j in range(1, tp):
            gated_copy(q, j).wait_recv()
        gated_own(q).wait()
        step = min(512, width)
        for c in range(width // step):
            part = slice(c * step, (c + 1) * step)
            premix[:, part] = jnp.dot(g_in[q], wo[:, part], preferred_element_type=F32)

        def norm(i, _):
            at = pl.multiple_of(i * 16, 16)
            x = premix[pl.ds(at, 16), :]
            scale = lax.rsqrt(jnp.mean(x * x, axis=-1, keepdims=True) + rms_eps)
            out[q, pl.ds(at, 16), :] = (x * scale * pgain[...]).astype(BF16)
            return 0

        lax.fori_loop(0, rows // 16, norm, 0)

    for q in range(seqs):
        own[q].wait()
    for load in loads:
        load.wait()

    def near(q, _):
        arrived(q, other)
        project(q, chip)
        return 0

    lax.fori_loop(0, seqs, near, 0)

    def far(q, _):
        for j in range(1, chips):
            who = lax.rem(chip + j, chips)
            mine, theirs = who * 2 + core, who * 2 + 1 - core
            arrived(q, mine)
            to_core(q, mine, False).start()
        if last > 0:
            @pl.when(q > 0)
            def _():
                for k in range(1, last):
                    take_state(q - 1, k)
                    send_state(q - 1, k + 1)
        for j in range(1, chips):
            who = lax.rem(chip + j, chips)
            arrived(q, who * 2 + 1 - core)
            project(q, who)
        make_state(q)
        if rounds:
            send_state(q, 0)
        inside(q)

        @pl.when(q > 0)
        def _():
            if last >= 0:
                take_state(q - 1, last)
            finish(q - 1)

        if last > 0:
            take_state(q, 0)
            send_state(q, 1)
        return 0

    lax.fori_loop(0, seqs, far, 0)

    end = seqs - 1
    if last > 0:
        for k in range(1, last):
            take_state(end, k)
            send_state(end, k + 1)
    if last >= 0:
        take_state(end, last)
    finish(end)

    def write(q, _):
        emit(q)
        return 0

    lax.fori_loop(0, seqs, write, 0)

    def drain(q, _):
        for j in range(1, chips):
            to_chip(q, j).wait_send()
            to_core(q, lax.rem(chip + j, chips) * 2 + core, False).wait_send()
        to_core(q, t, True).wait_send()
        for j in range(1, tp):
            gated_copy(q, j).wait_send()
        for k, d in enumerate(rounds):
            @pl.when(s + d < sp)
            def _():
                state_copy(q, k).wait_send()
        return 0

    lax.fori_loop(0, seqs, drain, 0)


def solution(mesh):
    tp, sp = mesh.shape["tp"], mesh.shape["sp"]

    def body(tok, gain, wq, wk, wv, wg, decay, ngain, wo, pgain):
        seqs, rows, width = tok.shape
        cols = wq.shape[1]
        heads = cols // HEAD_DIM
        length = rows * tp
        half = HEAD_DIM // 2
        inv = rope_base ** (-jnp.arange(half, dtype=F32) / half)
        inv = jnp.concatenate([inv, inv])[None, :]
        steps = max(1, (sp - 1).bit_length())
        dma = pltpu.SemaphoreType.DMA
        any_, vmem = pl.BlockSpec(memory_space=pl.ANY), pl.BlockSpec(memory_space=pltpu.VMEM)
        wide = pltpu.VMEM((seqs, length, cols), BF16)
        return pl.pallas_call(
            functools.partial(kernel, tp, sp),
            out_shape=jax.ShapeDtypeStruct(tok.shape, BF16),
            in_specs=[
                any_, vmem, any_, any_, any_, any_,
                pl.BlockSpec(memory_space=pltpu.SMEM), vmem, any_, vmem, vmem,
            ],
            out_specs=vmem,
            scratch_shapes=[
                pltpu.VMEM((seqs, length, width), BF16),
                pltpu.VMEM(wq.shape, BF16), pltpu.VMEM(wq.shape, BF16),
                pltpu.VMEM(wq.shape, BF16), pltpu.VMEM(wq.shape, BF16),
                pltpu.VMEM(wo.shape, BF16),
                pltpu.VMEM((2 * rows, width), BF16),
                pltpu.VMEM((length, HEAD_DIM), F32), pltpu.VMEM((length, HEAD_DIM), F32),
                pltpu.VMEM((heads, length, length), F32),
                wide, wide, wide, wide,
                pltpu.VMEM((seqs, length, cols), F32),
                pltpu.VMEM((seqs, heads, HEAD_DIM, HEAD_DIM), F32),
                pltpu.VMEM((seqs, heads, HEAD_DIM, HEAD_DIM), F32),
                pltpu.VMEM((seqs, steps, heads, HEAD_DIM, HEAD_DIM), BF16),
                pltpu.VMEM((seqs, steps, heads, HEAD_DIM, HEAD_DIM), BF16),
                wide,
                pltpu.VMEM((seqs, rows, cols * tp), BF16),
                pltpu.VMEM((rows, width), F32),
                dma((seqs, max(2, tp // 2))), dma((seqs, tp)), dma((seqs, tp)),
                dma((seqs, steps)), dma((seqs, steps)),
                dma((seqs, tp)), dma((seqs, tp)),
                dma((5,)), dma((seqs,)),
            ],
            compiler_params=pltpu.CompilerParams(
                collective_id=0, has_side_effects=True, vmem_limit_bytes=60 * 2**20
            ),
            name="retention",
        )(
            tok, gain[None, :], wq, wk, wv, wg, decay, ngain[None, :], wo, pgain[None, :], inv
        )

    placed = (
        P(None, ("sp", "tp"), None),
        P(),
        P(None, "tp"),
        P(None, "tp"),
        P(None, "tp"),
        P(None, "tp"),
        P("tp"),
        P("tp"),
        P(),
        P(),
    )
    return jax.shard_map(
        body, mesh=mesh, in_specs=placed, out_specs=P(None, ("sp", "tp"), None), check_vma=False
    )
```

time: 251 us -> 77.6 us (0.31); the launches traced: 246 us -> 77.4 us
  waiting for transfers between devices: 109 us -> 0 us
  Pallas kernels: 0 us -> 73.6 us
  matrix products: 36.7 us -> 0 us
  blocking collectives: 31.1 us -> 0 us
  other arithmetic: 27.9 us -> 0.6 us
  local copies, waits for them, and re-layouts: 27.2 us -> 3.16 us
  between operations: 14.4 us -> 0.01 us
    all_gather x2 -> x0, waiting for transfers between devices: 109 us -> none  [the longest x1 57 us: body(): lax.all_gather(normed, 'tp', axis=1, tiled=True)]
    pallas_call x0 -> x1, Pallas kernels: none -> 73.6 us  [body(): pl.pallas_call(functools.partial(kernel, tp, sp), out_shape=jax.ShapeDtyp...]
    dot_general x15 -> x0, matrix products: 36.7 us -> none  [the longest x1 11.8 us: body(): jnp.einsum('kux,xt->kut', lax.all_gather(normed, 'tp', axis=1, tiled=True...]
    all_to_all x1 -> x0, blocking collectives: 16.7 us -> none  [body(): lax.all_to_all(gated, 'tp', split_axis=1, concat_axis=2, tiled=True)]
    unnamed x1 -> x0, blocking collectives: 14.4 us -> none
    reshape x5 -> x0, local copies, waits for them, and re-layouts: 9.3 us -> none  [the longest x3 5.27 us: heads_of(): columns.reshape(seq_count, stretch, head_count, HEAD_DIM)]
    select_n x11 -> x0, other arithmetic: 8.64 us -> none  [the longest x7 8.26 us: lap(): jnp.where(position < mine, new, old)]
    convert_element_type x4 -> x0, other arithmetic: 6.19 us -> none  [the longest x1 2.6 us: body(): normed = (tok_f32 * lax.rsqrt(jnp.mean(tok_f32 * tok_f32, axis=-1, keepdi...]
  transfers between devices with their start and end apart: 2 -> 0, of which waited for: 2 -> 0; matrix products, arithmetic and copies ran while one was open for 3% -> 0% of each run, Pallas kernels for 0% -> 0%
where the time goes in v1:
time: 77.6 us; the launch traced here: 77.4 us
  Pallas kernels  73.6 us (95%)
  local copies, waits for them, and re-layouts  3.16 us (4%)
    pallas_call x1, Pallas kernels, body(): pl.pallas_call(functools.partial(kernel, tp, sp), out_shape=jax.ShapeDtyp...  73.6 us
    unnamed x1, local copies, waits for them, and re-layouts  3.16 us

profile of v1, /device:TPU:25, one launch (start us, length us, event | category | flops | bytes accessed | tf_op | source)
XLA Modules:
  0.0 77.4 jit_solution(4807767264581981762)
XLA Ops:
  0.0 0.6 maximum_bitcast_fusion.inv
  0.6 73.6 %retention.1 = bf16[4,128,2048]{2,1,0:T(8,128)(2,1)} custom-call(bf16[4,128,2048]{2,1,0:T(8,128)(2,1)} %tok.1, f32[1,2048]{1,0:T(1,128)} %bitcast.5, bf16[2048,256]{1,0:T(8,128)(2,1)} %wq_h.1, bf16[2048,256]{1,0:T(8,128)(2,1)} %wk_h.1, bf16[2048,256]{1,0:T(8,128)(2,1)} %wv_h.1, bf16[2048,256]{1,0:T(8,128)(2,1)} %wg_h.1, f32[2]{0:T(128)} %decay.1, ...), custom_call_target="tpu_custom_call" | custom-call | tf_op jit(solution)/shard_map/retention/pallas_call | solution.py:338
  74.2 3.2 %copy.12 = bf16[4,128,2048]{2,1,0:T(8,128)(2,1)} copy(bf16[4,128,2048]{2,1,0:T(8,128)(2,1)} %retention.1) | data formatting | bytes 4194304
  (1 shorter events, 0.0 us)

commit v2 on v1

--- a/solution.py
+++ b/solution.py
@@ -21,9 +21,9 @@
 
 def kernel(
     tp, sp,
-    tok, gain, wq_h, wk_h, wv_h, wg_h, decay, ngain, wo_h, pgain, inv,
+    tok, gain_h, wq_h, wk_h, wv_h, wg_h, decay, ngain_h, wo_h, pgain_h, inv_h,
     out,
-    gath, wq, wk, wv, wg, wo, nb, cosv, sinv, mask, qs, ks, vs, gs,
+    gain, ngain, pgain, inv, gath, wq, wk, wv, wg, wo, nb, cosv, sinv, mask, qs, ks, vs, gs,
     within, state, excl, st_out, st_in, g_out, g_in, premix,
     x_send, p_send, t_recv, s_send, s_recv, g_send, g_recv, w_sem, own_sem,
 ):
@@ -91,12 +91,16 @@
     loads = [
         pltpu.make_async_copy(a, b, w_sem.at[i])
         for i, (a, b) in enumerate(
-            ((wq_h, wq), (wk_h, wk), (wv_h, wv), (wg_h, wg), (wo_h, wo))
+            (
+                (inv_h, inv), (gain_h, gain), (ngain_h, ngain), (pgain_h, pgain),
+                (wk_h, wk), (wv_h, wv), (wq_h, wq), (wg_h, wg), (wo_h, wo),
+            )
         )
     ]
     for load in loads:
         load.start()
 
+    loads[0].wait()
     place = (s * length + lax.broadcasted_iota(jnp.int32, (length, HEAD_DIM), 0)).astype(F32)
     angle = place * inv[...]
     cosv[...] = jnp.cos(angle)
@@ -120,20 +124,22 @@
     def head(h):
         return slice(h * HEAD_DIM, (h + 1) * HEAD_DIM)
 
-    def project(q, which):
-        base = pl.multiple_of(which * pair, pair)
+    def normalise(q, who):
+        base = pl.multiple_of(who * rows, rows)
 
         def norm(i, _):
-            at = pl.multiple_of(i * 16, 16)
-            x = gath[q, pl.ds(pl.multiple_of(base + at, 16), 16), :].astype(F32)
+            at = pl.multiple_of(base + i * 16, 16)
+            x = gath[q, pl.ds(at, 16), :].astype(F32)
             scale = lax.rsqrt(jnp.mean(x * x, axis=-1, keepdims=True) + rms_eps)
             nb[pl.ds(at, 16), :] = (x * scale * gain[...]).astype(BF16)
             return 0
 
-        lax.fori_loop(0, pair // 16, norm, 0)
-        span = pl.ds(base, pair)
-        for w, dest, kind in ((wk, ks, 2), (wv, vs, 0), (wq, qs, 1), (wg, gs, 0)):
-            r = jnp.dot(nb[...], w[...], preferred_element_type=F32).astype(BF16)
+        lax.fori_loop(0, rows // 16, norm, 0, unroll=2)
+
+    def project(q, which, parts):
+        span = pl.ds(pl.multiple_of(which * pair, pair), pair)
+        for w, dest, kind in parts:
+            r = jnp.dot(nb[span, :], w[...], preferred_element_type=F32).astype(BF16)
             if kind == 0:
                 dest[q, span, :] = r
             else:
@@ -143,6 +149,9 @@
                     if kind == 2:
                         x = x * HEAD_DIM ** (-0.5)
                     dest[q, span, head(h)] = x.astype(BF16)
+
+    first = ((wk, ks, 2), (wv, vs, 0))
+    second = ((wq, qs, 1), (wg, gs, 0))
 
     def send_state(q, k):
         for h in range(heads):
@@ -189,12 +198,11 @@
                     weight, vs[q, upto, head(h)], preferred_element_type=F32
                 )
 
-    def gated_copy(q, j):
-        dest = lax.rem(t + j, tp)
+    def gated_copy(q, dest, source):
         return pltpu.make_async_remote_copy(
             g_out.at[q, pl.ds(pl.multiple_of(dest * rows, rows), rows), :],
-            g_in.at[q, :, pl.ds(pl.multiple_of(t * cols, cols), cols)],
-            g_send.at[q, j], g_recv.at[q, j],
+            g_in.at[q, :, pl.ds(pl.multiple_of(source * cols, cols), cols)],
+            g_send.at[q, dest], g_recv.at[q, source],
             device_id={"tp": dest}, device_id_type=MESH,
         )
 
@@ -202,37 +210,47 @@
         return pltpu.make_async_copy(
             g_out.at[q, pl.ds(pl.multiple_of(t * rows, rows), rows), :],
             g_in.at[q, :, pl.ds(pl.multiple_of(t * cols, cols), cols)],
-            g_recv.at[q, 0],
-        )
+            g_recv.at[q, t],
+        )
+
+    def members(j):
+        base = lax.rem(chip + j, chips) * 2
+        return base + core, base + 1 - core
 
     def finish(q):
-        for h in range(heads):
-            memory = excl[q, h].astype(BF16)
-            for i in range(length // SUB):
-                here = slice(i * SUB, (i + 1) * SUB)
-                spot = i * SUB + 1 + lax.broadcasted_iota(jnp.int32, (SUB, HEAD_DIM), 0)
+        for dest in [d for j in range(1, chips) for d in members(j)] + [other, t]:
+            here = pl.ds(pl.multiple_of(dest * rows, rows), rows)
+            spot = dest * rows + 1 + lax.broadcasted_iota(jnp.int32, (rows, HEAD_DIM), 0)
+            for h in range(heads):
                 reach = jnp.exp(decay[h] * spot.astype(F32))
                 query = (qs[q, here, head(h)].astype(F32) * reach).astype(BF16)
                 kept = within[q, here, head(h)] + jnp.dot(
-                    query, memory, preferred_element_type=F32
+                    query, excl[q, h].astype(BF16), preferred_element_type=F32
                 )
                 kept = kept - jnp.mean(kept, axis=-1, keepdims=True)
                 spread = jnp.mean(kept * kept, axis=-1, keepdims=True)
                 normal = kept * lax.rsqrt(spread + group_eps) * ngain[:, head(h)]
                 gate = gs[q, here, head(h)].astype(F32)
                 g_out[q, here, head(h)] = (normal * (gate * jax.nn.sigmoid(gate))).astype(BF16)
-        for j in range(1, tp):
-            gated_copy(q, j).start()
-        gated_own(q).start()
+            if dest is t:
+                gated_own(q).start()
+            else:
+                gated_copy(q, dest, t).start()
 
     def emit(q):
-        for j in range(1, tp):
-            gated_copy(q, j).wait_recv()
-        gated_own(q).wait()
         step = min(512, width)
-        for c in range(width // step):
-            part = slice(c * step, (c + 1) * step)
-            premix[:, part] = jnp.dot(g_in[q], wo[:, part], preferred_element_type=F32)
+        for j in range(chips):
+            if j == 0:
+                gated_own(q).wait()
+                gated_copy(q, other, other).wait_recv()
+            else:
+                for source in members(j):
+                    gated_copy(q, other, source).wait_recv()
+            span = pl.ds(pl.multiple_of(lax.rem(chip + j, chips) * 2 * cols, 2 * cols), 2 * cols)
+            for c in range(width // step):
+                part = slice(c * step, (c + 1) * step)
+                term = jnp.dot(g_in[q, :, span], wo[span, part], preferred_element_type=F32)
+                premix[:, part] = term if j == 0 else premix[:, part] + term
 
         def norm(i, _):
             at = pl.multiple_of(i * 16, 16)
@@ -241,24 +259,25 @@
             out[q, pl.ds(at, 16), :] = (x * scale * pgain[...]).astype(BF16)
             return 0
 
-        lax.fori_loop(0, rows // 16, norm, 0)
+        lax.fori_loop(0, rows // 16, norm, 0, unroll=2)
 
     for q in range(seqs):
         own[q].wait()
-    for load in loads:
+    for load in loads[1:]:
         load.wait()
 
     def near(q, _):
+        normalise(q, t)
         arrived(q, other)
-        project(q, chip)
+        normalise(q, other)
+        project(q, chip, first + second)
         return 0
 
     lax.fori_loop(0, seqs, near, 0)
 
     def far(q, _):
         for j in range(1, chips):
-            who = lax.rem(chip + j, chips)
-            mine, theirs = who * 2 + core, who * 2 + 1 - core
+            mine, _ = members(j)
             arrived(q, mine)
             to_core(q, mine, False).start()
         if last > 0:
@@ -268,12 +287,19 @@
                     take_state(q - 1, k)
                     send_state(q - 1, k + 1)
         for j in range(1, chips):
-            who = lax.rem(chip + j, chips)
-            arrived(q, who * 2 + 1 - core)
-            project(q, who)
+            mine, theirs = members(j)
+            normalise(q, mine)
+            arrived(q, theirs)
+            normalise(q, theirs)
+            project(q, lax.rem(chip + j, chips), first)
         make_state(q)
         if rounds:
             send_state(q, 0)
+        for j in range(1, chips):
+            project(q, lax.rem(chip + j, chips), second)
+        if last > 0:
+            take_state(q, 0)
+            send_state(q, 1)
         inside(q)
 
         @pl.when(q > 0)
@@ -281,28 +307,25 @@
             if last >= 0:
                 take_state(q - 1, last)
             finish(q - 1)
-
-        if last > 0:
-            take_state(q, 0)
-            send_state(q, 1)
         return 0
 
     lax.fori_loop(0, seqs, far, 0)
 
+    def write(q, _):
+        emit(q)
+        return 0
+
     end = seqs - 1
-    if last > 0:
-        for k in range(1, last):
-            take_state(end, k)
-            send_state(end, k + 1)
+    for k in range(1, last):
+        take_state(end, k)
+        send_state(end, k + 1)
+    done = min(2, end)
+    lax.fori_loop(0, done, write, 0)
     if last >= 0:
         take_state(end, last)
     finish(end)
 
-    def write(q, _):
-        emit(q)
-        return 0
-
-    lax.fori_loop(0, seqs, write, 0)
+    lax.fori_loop(done, seqs, write, 0)
 
     def drain(q, _):
         for j in range(1, chips):
@@ -310,7 +333,7 @@
             to_core(q, lax.rem(chip + j, chips) * 2 + core, False).wait_send()
         to_core(q, t, True).wait_send()
         for j in range(1, tp):
-            gated_copy(q, j).wait_send()
+            gated_copy(q, lax.rem(t + j, tp), t).wait_send()
         for k, d in enumerate(rounds):
             @pl.when(s + d < sp)
             def _():
@@ -329,26 +352,28 @@
         heads = cols // HEAD_DIM
         length = rows * tp
         half = HEAD_DIM // 2
-        inv = rope_base ** (-jnp.arange(half, dtype=F32) / half)
-        inv = jnp.concatenate([inv, inv])[None, :]
+        inv = np.float32(rope_base) ** (-np.arange(half, dtype=np.float32) / half)
+        inv = jnp.asarray(np.concatenate([inv, inv])[None, :], F32)
         steps = max(1, (sp - 1).bit_length())
         dma = pltpu.SemaphoreType.DMA
-        any_, vmem = pl.BlockSpec(memory_space=pl.ANY), pl.BlockSpec(memory_space=pltpu.VMEM)
+        hbm, vmem = pl.BlockSpec(memory_space=pltpu.HBM), pl.BlockSpec(memory_space=pltpu.VMEM)
         wide = pltpu.VMEM((seqs, length, cols), BF16)
         return pl.pallas_call(
             functools.partial(kernel, tp, sp),
             out_shape=jax.ShapeDtypeStruct(tok.shape, BF16),
             in_specs=[
-                any_, vmem, any_, any_, any_, any_,
-                pl.BlockSpec(memory_space=pltpu.SMEM), vmem, any_, vmem, vmem,
+                hbm, hbm, hbm, hbm, hbm, hbm,
+                pl.BlockSpec(memory_space=pltpu.SMEM), hbm, hbm, hbm, hbm,
             ],
             out_specs=vmem,
             scratch_shapes=[
+                pltpu.VMEM((1, width), F32), pltpu.VMEM((1, cols), F32),
+                pltpu.VMEM((1, width), F32), pltpu.VMEM((1, HEAD_DIM), F32),
                 pltpu.VMEM((seqs, length, width), BF16),
                 pltpu.VMEM(wq.shape, BF16), pltpu.VMEM(wq.shape, BF16),
                 pltpu.VMEM(wq.shape, BF16), pltpu.VMEM(wq.shape, BF16),
                 pltpu.VMEM(wo.shape, BF16),
-                pltpu.VMEM((2 * rows, width), BF16),
+                pltpu.VMEM((length, width), BF16),
                 pltpu.VMEM((length, HEAD_DIM), F32), pltpu.VMEM((length, HEAD_DIM), F32),
                 pltpu.VMEM((heads, length, length), F32),
                 wide, wide, wide, wide,
@@ -363,10 +388,10 @@
                 dma((seqs, max(2, tp // 2))), dma((seqs, tp)), dma((seqs, tp)),
                 dma((seqs, steps)), dma((seqs, steps)),
                 dma((seqs, tp)), dma((seqs, tp)),
-                dma((5,)), dma((seqs,)),
+                dma((9,)), dma((seqs,)),
             ],
             compiler_params=pltpu.CompilerParams(
-                collective_id=0, has_side_effects=True, vmem_limit_bytes=60 * 2**20
+                collective_id=0, has_side_effects=True, vmem_limit_bytes=59 * 2**20
             ),
             name="retention",
         )(

time: 77.6 us -> 75.8 us (0.977); the launches traced: 77.4 us -> 74.3 us
  Pallas kernels: 73.6 us -> 71.1 us
    pallas_call x1, Pallas kernels: 73.6 us -> 71.1 us  [body(): pl.pallas_call(functools.partial(kernel, tp, sp), out_shape=jax.ShapeDtyp...]
where the time goes in v2:
time: 75.8 us; the launch traced here: 74.3 us
  Pallas kernels  71.1 us (94%)
  local copies, waits for them, and re-layouts  3.16 us (4%)
    pallas_call x1, Pallas kernels, body(): pl.pallas_call(functools.partial(kernel, tp, sp), out_shape=jax.ShapeDtyp...  71.1 us
    unnamed x1, local copies, waits for them, and re-layouts  3.16 us

profile of v2, /device:TPU:25, one launch (start us, length us, event | category | flops | bytes accessed | tf_op | source)
XLA Modules:
  0.0 74.3 jit_solution(17188380535637859954)
XLA Ops:
  0.0 71.1 %retention.1 = bf16[4,128,2048]{2,1,0:T(8,128)(2,1)} custom-call(bf16[4,128,2048]{2,1,0:T(8,128)(2,1)} %tok.1, f32[1,2048]{1,0:T(1,128)} %bitcast.3, bf16[2048,256]{1,0:T(8,128)(2,1)} %wq_h.1, bf16[2048,256]{1,0:T(8,128)(2,1)} %wk_h.1, bf16[2048,256]{1,0:T(8,128)(2,1)} %wv_h.1, bf16[2048,256]{1,0:T(8,128)(2,1)} %wg_h.1, f32[2]{0:T(128)} %decay.1, ...), custom_call_target="tpu_custom_call" | custom-call | tf_op jit(solution)/shard_map/retention/pallas_call | solution.py:361
  71.1 3.2 %copy.13 = bf16[4,128,2048]{2,1,0:T(8,128)(2,1)} copy(bf16[4,128,2048]{2,1,0:T(8,128)(2,1)} %retention.1) | data formatting | bytes 4194304
